TPU v7x, 128 devices: a whole 4x4x4 slice. The times are simulated.
128 devices in a mesh: sp: 16 (over z, y), tp: 8 (over x, core).
Axes of the slice: x: 4, y: 4, z: 4, core: 2. Of those that a mesh axis runs over, the one named last changes fastest.
Arguments:
- queries: bfloat16 [12288, 2048], P('sp', 'tp'), may hold values from -11 to 11
- key_rows: bfloat16 [12288, 2048], P('sp', 'tp'), may hold values from -4.5 to 4.5
- value_rows: bfloat16 [12288, 2048], P('sp', 'tp'), may hold values from -6 to 6
- log_forget: float32 [12288, 32], P('sp', 'tp'), may hold values from -1477.56 to 0, as said below
- stream_in: bfloat16 [12288, 2048], P('sp'), may hold values from -6 to 6
- out_weight: bfloat16 [2048, 2048], P('tp'), may hold values from -0.52734375 to 0.52734375
- mix_gain: float32 [2048], replicated, may hold values from 0.1 to 1.9
- mix_bias: float32 [2048], replicated, may hold values from -3 to 3
- gate_weight: bfloat16 [2048, 5632], P('sp', 'tp'), may hold values from -0.125 to 0.125
- up_weight: bfloat16 [2048, 5632], P('sp', 'tp'), may hold values from -0.125 to 0.125
- down_weight: bfloat16 [5632, 2048], P('tp', 'sp'), may hold values from -0.15917969 to 0.15917969
- ffn_gain: float32 [2048], replicated, may hold values from 0.1 to 1.9
- ffn_bias: float32 [2048], replicated, may hold values from -3 to 3
Outputs:
- layer_out: bfloat16 [12288, 2048], P(('sp', 'tp'))
Inputs may be any that keep to these rules, and one draw needn't show every extreme that they name: `log_forget`: each column never rises along the positions.
All inputs are finite; a program needn't handle non-finite values.
Results may differ from a plain program's by a relative error of at most 0.015.
Values may be sent and summed in bfloat16 or wider, within the bound.
A program may use at most 128 MiB of HBM per device.

v0:
```python
import jax
import jax.numpy as jnp
from jax import lax
from jax.sharding import PartitionSpec as P

ALPHA = 8.0**0.25
EPSILON = 1e-05


def laid_out(pieces, dim):
    lengths = list(pieces.shape[1:])
    lengths[dim] *= pieces.shape[0]
    return jnp.moveaxis(pieces, 0, dim).reshape(lengths)


def from_everyone(value, axis):
    copies = jnp.broadcast_to(value, (lax.axis_size(axis), *value.shape))
    return lax.all_to_all(copies, axis, split_axis=0, concat_axis=0, tiled=True)


def gathered_copies(value, axis, dim):
    return laid_out(from_everyone(value, axis), dim)


def in_one_piece(arrays, axis, dim, along):
    ends, at = ([], 0)
    for a in arrays[:-1]:
        at += a.shape[along]
        ends.append(at)
    both = jnp.concatenate(arrays, axis=along)
    return tuple(jnp.split(lax.all_gather(both, axis, axis=dim, tiled=True), ends, axis=along))


def in_blocks(value, dim, count):
    before, after = (value.shape[:dim], value.shape[dim + 1 :])
    return jnp.moveaxis(value.reshape(*before, count, -1, *after), dim, 0)


def sum_at_owner(value, axis, dim):
    pieces = in_blocks(value, dim, lax.axis_size(axis))
    arrived = lax.all_to_all(pieces, axis, split_axis=0, concat_axis=0, tiled=True)
    return arrived.astype(jnp.float32).sum(axis=0)


def layer_norm(matrix, norm_gain, norm_shift):
    centred = matrix - jnp.mean(matrix, axis=-1, keepdims=True)
    spread = jnp.mean(centred * centred, axis=-1, keepdims=True)
    return centred * lax.rsqrt(spread + EPSILON) * norm_gain + norm_shift


def attend(queries, key_rows, value_rows, log_forget):
    length, row_width = queries.shape
    head_count = log_forget.shape[1]
    head_dim = row_width // head_count
    score_scale = head_dim ** (-0.5)
    first_pos = lax.axis_index("sp") * length
    last_pos = first_pos + length
    query_heads = queries.reshape(length, head_count, head_dim)
    query_gates = log_forget.T
    query_pos = first_pos + jnp.arange(length, dtype=jnp.int32)
    gates_all = gathered_copies(log_forget, "sp", 0)
    initial = (
        jnp.full((head_count, length), -1e30, jnp.float32),
        jnp.zeros((head_count, length), jnp.float32),
        jnp.zeros((length, head_count, head_dim), jnp.float32),
    )
    running = initial
    key_piece, value_piece = in_one_piece((key_rows, value_rows), "sp", 0, 1)
    piece_len = key_piece.shape[0]
    shards = piece_len // length
    group_size = max(
        [
            count_try
            for count_try in range(1, shards + 1)
            if shards % count_try == 0 and count_try * length <= max(length, 512)
        ]
    )
    block_len = group_size * length
    blocks = piece_len // block_len
    key_blocks = key_piece.reshape(blocks, block_len, head_count, head_dim)
    value_blocks = value_piece.reshape(blocks, block_len, head_count, head_dim)
    gate_blocks = gates_all.reshape(blocks, block_len, head_count)
    block_starts = block_len * jnp.arange(blocks, dtype=jnp.int32)

    def one_block(running_state, packed):
        key_block, value_block, gate_block, block_start = packed

        def compute(state_in):
            highest, totals, weighted = state_in
            scores = (
                jnp.einsum(
                    "qhd,khd->hqk", query_heads, key_block, preferred_element_type=jnp.float32
                )
                * score_scale
            )
            scores = scores + query_gates[:, :, None] - gate_block.T[:, None, :]
            key_pos = block_start + jnp.arange(block_len, dtype=jnp.int32)
            allowed = (key_pos[None, :] <= query_pos[:, None])[None]
            masked = jnp.where(allowed, scores, -1e30)
            new_high = jnp.maximum(highest, jnp.max(masked, axis=2))
            weights = jnp.where(allowed, jnp.exp(masked - new_high[:, :, None]), 0.0)
            factor = jnp.exp(highest - new_high)
            totals = totals * factor + jnp.sum(weights, axis=2)
            weighted = weighted * factor.T[:, :, None] + jnp.einsum(
                "hqk,khd->qhd",
                weights.astype(jnp.bfloat16),
                value_block,
                preferred_element_type=jnp.float32,
            )
            return (new_high, totals, weighted)

        def keep_state(state_in):
            return state_in

        return (lax.cond(block_start < last_pos, compute, keep_state, running_state), None)

    running, unused = lax.scan(
        one_block, running, (key_blocks, value_blocks, gate_blocks, block_starts)
    )
    highest, totals, weighted = running
    return (weighted / totals.T[:, :, None]).reshape(length, row_width).astype(jnp.bfloat16)


def body(
    queries,
    key_rows,
    value_rows,
    log_forget,
    stream_in,
    out_weight,
    mix_gain,
    mix_bias,
    gate_weight,
    up_weight,
    down_weight,
    ffn_gain,
    ffn_bias,
):
    attended = attend(queries, key_rows, value_rows, log_forget)
    length = attended.shape[0]
    own_rows = length // lax.axis_size("tp")
    offset = lax.axis_index("tp") * own_rows
    summed = sum_at_owner(
        jnp.dot(attended, out_weight, preferred_element_type=jnp.float32).astype(jnp.bfloat16),
        "tp",
        0,
    )
    mix_out = lax.optimization_barrier(summed.astype(jnp.bfloat16)).astype(jnp.float32)
    stream_own = lax.dynamic_slice_in_dim(stream_in, offset, own_rows, 0)
    normed = layer_norm(
        ALPHA * stream_own.astype(jnp.float32) + mix_out, mix_gain, mix_bias
    ).astype(jnp.bfloat16)
    gathered = lax.all_gather(normed, "tp", axis=0, tiled=True)
    pieces = in_one_piece((gate_weight, up_weight), "sp", 0, 1)
    gate_part = jnp.dot(gathered, pieces[0], preferred_element_type=jnp.float32)
    up_part = jnp.dot(gathered, pieces[1], preferred_element_type=jnp.float32)
    hidden = (jax.nn.silu(gate_part) * up_part).astype(jnp.bfloat16)
    partial_terms = jnp.dot(
        hidden,
        lax.all_gather(down_weight, "sp", axis=1, tiled=True),
        preferred_element_type=jnp.float32,
    )
    lowered = lax.psum_scatter(
        partial_terms.astype(jnp.bfloat16), "tp", scatter_dimension=0, tiled=True
    ).astype(jnp.float32)
    lowered = lax.optimization_barrier(lowered.astype(jnp.bfloat16)).astype(jnp.float32)
    result = layer_norm(ALPHA * normed.astype(jnp.float32) + lowered, ffn_gain, ffn_bias)
    return result.astype(jnp.bfloat16)


def solution(mesh):
    placed = (
        P("sp", "tp"),
        P("sp", "tp"),
        P("sp", "tp"),
        P("sp", "tp"),
        P("sp", None),
        P("tp", None),
        P(),
        P(),
        P("sp", "tp"),
        P("sp", "tp"),
        P("tp", "sp"),
        P(),
        P(),
    )
    return jax.shard_map(
        body, mesh=mesh, in_specs=placed, out_specs=P(("sp", "tp"), None), check_vma=False
    )
```

profile of v0, /device:TPU:0, one launch (start us, length us, event | category | flops | bytes accessed | tf_op | source)
XLA Modules:
  0.0 604.3 jit_solution(4880820120093457124)
XLA Ops:
  6.5 2.2 pad_maximum_fusion
  12.0 8.2 %all-to-all-start = ((f32[16,768,4]{1,2,0:T(4,128)}), f32[16,768,4]{1,2,0:T(4,128)S(1)}, u32[]{:S(2)}, u32[]{:S(2)}) async-start(f32[16,768,4]{1,2,0:T(4,128)} %broadcast_in_dim.56), calls=%async_computation | async-start | bytes 393216 | tf_op jit(solution)/shard_map/all_to_all | solution.py:18
  21.4 80.5 %all-gather.5.cloned.1.call-done = bf16[12288,512]{1,0:T(8,128)(2,1)} async-done(((bf16[768,512]{1,0:T(8,128)(2,1)}), bf16[12288,512]{1,0:T(8,128)(2,1)}) %all-gather.5.cloned.1.call-update) | async-done | bytes 12582928 | tf_op jit(solution)/shard_map/all_gather | solution.py:31
  101.9 10.1 %fusion.36 = (bf16[12288,256]{1,0:T(8,128)(2,1)}, bf16[12288,256]{1,0:T(8,128)(2,1)}) fusion(bf16[12288,512]{1,0:T(8,128)(2,1)} %all-gather.5.cloned.1.call-done), kind=kLoop, calls=%fused_computation.51 | loop fusion | bytes 25165824 | tf_op jit(solution)/shard_map/split | solution.py:31
  112.0 18.8 %reshape.82 = bf16[16,768,4,64]{3,2,1,0:T(4,128)(2,1)} reshape(bf16[12288,256]{1,0:T(8,128)(2,1)} %get-tuple-element.249) | data formatting | bytes 12582912 | tf_op jit(solution)/shard_map/reshape | solution.py:80
  130.8 18.1 %copy.20 = bf16[16,768,4,64]{1,3,2,0:T(8,128)(2,1)} copy(bf16[16,768,4,64]{3,2,1,0:T(4,128)(2,1)} %reshape.82) | data formatting | bytes 12582912
  148.9 18.8 %reshape.83 = bf16[16,768,4,64]{3,2,1,0:T(4,128)(2,1)} reshape(bf16[12288,256]{1,0:T(8,128)(2,1)} %get-tuple-element.248) | data formatting | bytes 12582912 | tf_op jit(solution)/shard_map/reshape | solution.py:81
  167.6 18.1 %copy.21 = bf16[16,768,4,64]{1,3,2,0:T(8,128)(2,1)} copy(bf16[16,768,4,64]{3,2,1,0:T(4,128)(2,1)} %reshape.83) | data formatting | bytes 12582912
  185.8 33.5 %while.15 = (s32[]{:T(128)}, f32[4,768]{1,0:T(4,128)S(1)}, f32[4,768]{1,0:T(4,128)S(1)}, f32[768,4,64]{0,2,1:T(8,128)S(1)}, s32[16]{0:T(128)S(1)}, /*index=5*/s3...) while((s32[]{:T(128)}, f32[4,768]{1,0:T(4,128)S(1)}, ...), condition=%wide.region_5.6_spmd.clone, body=%wide.region_0.5_spmd.clone.sunk | while | flops 649800192 | bytes 33738040 | solution.py:117
  187.1 13.1 %conditional.3 = ((f32[4,768]{1,0:T(4,128)S(1)}, f32[4,768]{1,0:T(4,128)S(1)}, f32[768,4,64]{0,2,1:T(8,128)S(1)})) conditional(s32[]{:T(128)} %convert_element_type.100, (f32[4,768]{1,0:T(4,128)S(1)}, f32[4,768]{1,0:T(4,128)S(1)}, f32[768,4,64]{0,2,1:T(8,128)S(1)}) %tuple.41, (s32[]{:T(128)}, s32[]{:T(128)}, bf16[16,768,4,64]{1,3,2,0:T(8,128)(2,1)}, ...), branch_computations={%region_1.1_spmd, %region_2.4_spmd} | conditional | flops 649800192 | bytes 33734700 | solution.py:115
  188.2 3.9 fusion.4
  192.0 4.6 fusion.11
  196.6 3.5 fusion.3
  219.4 2.7 convolution_convert_fusion.1
  222.1 4.6 all-to-all-start.1
  226.9 38.2 %all-to-all-done.1 = bf16[8,96,2048]{2,1,0:T(8,128)(2,1)} async-done(((bf16[8,96,2048]{2,1,0:T(8,128)(2,1)}), bf16[8,96,2048]{2,1,0:T(8,128)(2,1)}, u32[]{:S(2)}, u32[]{:S(2)}) %all-to-all-start.1) | async-done | bytes 3145760 | tf_op jit(solution)/shard_map/all_to_all | solution.py:41
  265.1 2.5 reduce_sum.59
  270.2 2.0 add_convert_fusion.1
  272.8 220.0 %all-gather.7.cloned.1.call-done = bf16[768,2048]{1,0:T(8,128)(2,1)} async-done(((bf16[96,2048]{1,0:T(8,128)(2,1)}), bf16[768,2048]{1,0:T(8,128)(2,1)}) %all-gather.7.cloned.1.call-update) | async-done | bytes 3145744 | tf_op jit(solution)/shard_map/all_gather | solution.py:153
  492.8 6.5 %fusion.27 = f32[768,704]{0,1:T(8,128)} fusion(bf16[768,2048]{1,0:T(8,128)(2,1)} %all-gather.7.cloned.1.call-done, bf16[2048,1408]{0,1:T(8,128)(2,1)} %all-gather.9.cloned.1.call-done), kind=kOutput, calls=%fused_computation.31 | convolution fusion | flops 2214592512 | bytes 8192000 | tf_op jit(solution)/shard_map/dot_general | solution.py:155
  499.3 46.2 %all-gather.11.cloned.1.call-done = bf16[704,2048]{1,0:T(8,128)(2,1)} async-done(((bf16[704,128]{1,0:T(8,128)(2,1)}), bf16[704,2048]{1,0:T(8,128)(2,1)}) %all-gather.11.cloned.1.call-update) | async-done | bytes 2883600 | tf_op jit(solution)/shard_map/all_gather | solution.py:160
  545.5 12.4 %convolution_convert_fusion = bf16[768,2048]{1,0:T(8,128)(2,1)} fusion(bf16[704,2048]{1,0:T(8,128)(2,1)} %all-gather.11.cloned.1.call-done, f32[768,704]{0,1:T(8,128)} %fusion.27, bf16[768,2048]{1,0:T(8,128)(2,1)} %all-gather.7.cloned.1.call-done, bf16[2048,1408]{0,1:T(8,128)(2,1)} %all-gather.9.cloned.1.call-done), kind=kOutput, calls=%fused_computation.27 | convolution fusion | flops 4434001920 | bytes 14221312 | tf_op jit(solution)/shard_map/dot_general | solution.py:158
  557.9 35.3 %reduce-scatter.2.cloned.1.call-done = bf16[96,2048]{1,0:T(8,128)(2,1)} async-done(((bf16[768,2048]{1,0:T(8,128)(2,1)}), bf16[96,2048]{1,0:T(8,128)(2,1)}) %reduce-scatter.2.cloned.1.call-update) | async-done | bytes 393232 | tf_op jit(solution)/shard_map/reduce_scatter | solution.py:163
  595.7 2.0 add_convert_fusion
  (95 shorter events, 21.2 us)
Async XLA Ops:
  6.5 212.9 %copy-start = (bf16[256,2048]{1,0:T(8,128)(2,1)S(1)}, bf16[256,2048]{1,0:T(8,128)(2,1)}, u32[]{:S(2)}) copy-start(bf16[256,2048]{1,0:T(8,128)(2,1)} %param.22) | copy-start | bytes 3145732
  6.5 95.4 %all-gather.5.cloned.1.call-start = ((), (), s32[]{:S(2)}) async-start(), calls=%async_computation.3 | async-start | bytes 13369344 | tf_op jit(solution)/shard_map/all_gather | solution.py:31
  8.8 264.1 %all-gather.9.cloned.1.call-start = ((), (), s32[]{:S(2)}) async-start(), calls=%async_computation.5 | async-start | bytes 6127616 | tf_op jit(solution)/shard_map/all_gather | solution.py:31
  12.0 173.7 %all-to-all-start = ((f32[16,768,4]{1,2,0:T(4,128)}), f32[16,768,4]{1,2,0:T(4,128)S(1)}, u32[]{:S(2)}, u32[]{:S(2)}) async-start(f32[16,768,4]{1,2,0:T(4,128)} %broadcast_in_dim.56), calls=%async_computation | async-start | bytes 393216 | tf_op jit(solution)/shard_map/all_to_all | solution.py:18
  167.6 18.2 %copy-start.2 = (f32[768,4]{0,1:T(4,128)S(1)}, f32[768,4]{0,1:T(4,128)}, u32[]{:S(2)}) copy-start(f32[768,4]{0,1:T(4,128)} %param.20) | copy-start | bytes 36868
  222.1 48.0 %copy-start.3 = (f32[2048]{0:T(1024)S(1)}, f32[2048]{0:T(1024)}, u32[]{:S(2)}) copy-start(f32[2048]{0:T(1024)} %param.24) | copy-start | bytes 24580
  222.1 48.0 %copy-start.4 = (f32[2048]{0:T(1024)S(1)}, f32[2048]{0:T(1024)}, u32[]{:S(2)}) copy-start(f32[2048]{0:T(1024)} %param.23) | copy-start | bytes 24580
  222.1 43.0 %all-to-all-start.1 = ((bf16[8,96,2048]{2,1,0:T(8,128)(2,1)}), bf16[8,96,2048]{2,1,0:T(8,128)(2,1)}, u32[]{:S(2)}, u32[]{:S(2)}) async-start(bf16[8,96,2048]{2,1,0:T(8,128)(2,1)} %bitcast.45), calls=%async_computation.1 | async-start | bytes 6291456 | tf_op jit(solution)/shard_map/all_to_all | solution.py:41
  226.7 266.1 %all-gather.7.cloned.1.call-start = ((), (), s32[]{:S(2)}) async-start(), calls=%async_computation.4 | async-start | bytes 3538944 | tf_op jit(solution)/shard_map/all_gather | solution.py:153
  272.2 273.3 %all-gather.11.cloned.1.call-start = ((), (), s32[]{:S(2)}) async-start(), calls=%async_computation.6 | async-start | bytes 3063808 | tf_op jit(solution)/shard_map/all_gather | solution.py:160
  272.8 320.4 %reduce-scatter.2.cloned.1.call-start = ((), (), s32[]{:S(2)}) async-start(), calls=%async_computation.7 | async-start | bytes 3538944 | tf_op jit(solution)/shard_map/reduce_scatter | solution.py:163
  499.3 93.9 %copy-start.1 = (bf16[96,2048]{1,0:T(8,128)(2,1)S(1)}, bf16[96,2048]{1,0:T(8,128)(2,1)}, u32[]{:S(2)}) copy-start(bf16[96,2048]{1,0:T(8,128)(2,1)} %add_convert_fusion.1) | copy-start | bytes 1179652
  499.3 96.4 %copy-start.5 = (f32[2048]{0:T(1024)S(1)}, f32[2048]{0:T(1024)}, u32[]{:S(2)}) copy-start(f32[2048]{0:T(1024)} %param.29) | copy-start | bytes 24580
  499.3 96.4 %copy-start.6 = (f32[2048]{0:T(1024)S(1)}, f32[2048]{0:T(1024)}, u32[]{:S(2)}) copy-start(f32[2048]{0:T(1024)} %param.28) | copy-start | bytes 24580
Sparse Core Ops, SparseCore 0:
  9.5 92.3 all-gather.4
  104.0 64.0 all-gather.8
  272.3 220.4 all-gather.6
  494.8 50.6 all-gather.10
  558.0 35.0 reduce-scatter.1
where the time goes:
time: 608 us; the launch traced here: 604 us
  waiting for transfers between devices  421 us (69%)
  local copies, waits for them, and re-layouts  95.9 us (16%)
  matrix products  30.1 us (5%)
  other arithmetic  20.1 us (3%)
  between operations  13.3 us (2%)
  starting transfers between devices  13.1 us (2%)
  loops' own time  11.1 us (2%)
    all_gather x1, waiting for transfers between devices, body(): gathered = lax.all_gather(normed, 'tp', axis=0, tiled=True)  220 us
    all_gather x2, waiting for transfers between devices, in_one_piece(): lax.all_gather(both, axis, axis=dim, tiled=True)  80.5 us
    all_gather x1, waiting for transfers between devices, body(): lax.all_gather(down_weight, 'sp', axis=1, tiled=True)  46.2 us
    all_to_all x1, waiting for transfers between devices, sum_at_owner(): lax.all_to_all(pieces, axis, split_axis=0, concat_axis=0, tiled=True)  38.2 us
    unnamed x17, local copies, waits for them, and re-layouts  37.4 us
    reduce_scatter x1, waiting for transfers between devices, body(): lax.psum_scatter(partial_terms.astype(jnp.bfloat16), 'tp', scatter_dimens...  35.3 us
    reshape x1, local copies, waits for them, and re-layouts, attend(): key_blocks = key_piece.reshape(blocks, block_len, head_count, head_dim)  18.8 us
    reshape x1, local copies, waits for them, and re-layouts, attend(): value_blocks = value_piece.reshape(blocks, block_len, head_count, head_dim)  18.8 us
  transfers between devices with their start and end apart: 7, of which 5 were waited for; matrix products, arithmetic and copies ran while one was open for 21% of the time, Pallas kernels for 0%

commit v1 on v0

--- a/solution.py
+++ b/solution.py
@@ -2,9 +2,19 @@
 import jax.numpy as jnp
 from jax import lax
 from jax.sharding import PartitionSpec as P
+from jax.lax import all_to_all, axis_size
 
 ALPHA = 8.0**0.25
 EPSILON = 1e-05
+
+
+def _meet_wires(inp, which_axis):
+    return jnp.concatenate(
+        all_to_all(
+            jnp.stack(axis_size(which_axis) * [inp]), which_axis, split_axis=0, concat_axis=0
+        ),
+        0,
+    )
 
 
 def laid_out(pieces, dim):
@@ -150,7 +160,7 @@
     normed = layer_norm(
         ALPHA * stream_own.astype(jnp.float32) + mix_out, mix_gain, mix_bias
     ).astype(jnp.bfloat16)
-    gathered = lax.all_gather(normed, "tp", axis=0, tiled=True)
+    gathered = _meet_wires(normed, "tp")
     pieces = in_one_piece((gate_weight, up_weight), "sp", 0, 1)
     gate_part = jnp.dot(gathered, pieces[0], preferred_element_type=jnp.float32)
     up_part = jnp.dot(gathered, pieces[1], preferred_element_type=jnp.float32)

time: 608 us -> 579 us (0.952)
  waiting for transfers between devices: 421 us -> 386 us
    all_gather x1 -> x0, waiting for transfers between devices: 220 us -> none  [body(): gathered = lax.all_gather(normed, 'tp', axis=0, tiled=True)]
    all_gather x1, waiting for transfers between devices: 46.2 us -> 152 us  [body(): lax.all_gather(down_weight, 'sp', axis=1, tiled=True)]
    reduce_scatter x1, waiting for transfers between devices: 35.3 us -> 76.4 us  [body(): lax.psum_scatter(partial_terms.astype(jnp.bfloat16), 'tp', scatter_dimens...]
    all_to_all x0 -> x1, waiting for transfers between devices: none -> 38.3 us  [_meet_wires(): all_to_all(jnp.stack(axis_size(which_axis) * [inp]), which_axis, split_ax...]
    unnamed x17 -> x15, local copies, waits for them, and re-layouts: 37.4 us -> 37.4 us
  transfers between devices with their start and end apart: 7 -> 7, of which waited for: 5 -> 5; matrix products, arithmetic and copies ran while one was open for 21% -> 22% of each run, Pallas kernels for 0% -> 0%
where the time goes in v1:
time: 579 us; the launch traced here: 575 us
  waiting for transfers between devices  386 us (67%)
  local copies, waits for them, and re-layouts  98.4 us (17%)
  matrix products  30.1 us (5%)
  other arithmetic  19.3 us (3%)
  starting transfers between devices  17.5 us (3%)
  between operations  13.3 us (2%)
  loops' own time  10.9 us (2%)
    all_gather x1, waiting for transfers between devices, body(): lax.all_gather(down_weight, 'sp', axis=1, tiled=True)  152 us
    all_gather x2, waiting for transfers between devices, in_one_piece(): lax.all_gather(both, axis, axis=dim, tiled=True)  80.5 us
    reduce_scatter x1, waiting for transfers between devices, body(): lax.psum_scatter(partial_terms.astype(jnp.bfloat16), 'tp', scatter_dimens...  76.4 us
    all_to_all x1, waiting for transfers between devices, _meet_wires(): all_to_all(jnp.stack(axis_size(which_axis) * [inp]), which_axis, split_ax...  38.3 us
    all_to_all x1, waiting for transfers between devices, sum_at_owner(): lax.all_to_all(pieces, axis, split_axis=0, concat_axis=0, tiled=True)  37.7 us
    unnamed x15, local copies, waits for them, and re-layouts  37.4 us
    reshape x1, local copies, waits for them, and re-layouts, attend(): value_blocks = value_piece.reshape(blocks, block_len, head_count, head_dim)  18.8 us
    reshape x1, local copies, waits for them, and re-layouts, attend(): key_blocks = key_piece.reshape(blocks, block_len, head_count, head_dim)  18.8 us
  transfers between devices with their start and end apart: 7, of which 5 were waited for; matrix products, arithmetic and copies ran while one was open for 22% of the time, Pallas kernels for 0%

profile of v1, /device:TPU:0, one launch (start us, length us, event | category | flops | bytes accessed | tf_op | source)
XLA Modules:
  0.0 575.3 jit_solution(741586966160169847)
XLA Ops:
  6.5 2.2 pad_maximum_fusion
  12.0 8.2 %all-to-all-start = ((f32[16,768,4]{1,2,0:T(4,128)}), f32[16,768,4]{1,2,0:T(4,128)S(1)}, u32[]{:S(2)}, u32[]{:S(2)}) async-start(f32[16,768,4]{1,2,0:T(4,128)} %broadcast_in_dim.56), calls=%async_computation | async-start | bytes 393216 | tf_op jit(solution)/shard_map/all_to_all | solution.py:28
  21.4 80.5 %all-gather.4.cloned.1.call-done = bf16[12288,512]{1,0:T(8,128)(2,1)} async-done(((bf16[768,512]{1,0:T(8,128)(2,1)}), bf16[12288,512]{1,0:T(8,128)(2,1)}) %all-gather.4.cloned.1.call-update) | async-done | bytes 12582928 | tf_op jit(solution)/shard_map/all_gather | solution.py:41
  101.9 10.1 %fusion.36 = (bf16[12288,256]{1,0:T(8,128)(2,1)}, bf16[12288,256]{1,0:T(8,128)(2,1)}) fusion(bf16[12288,512]{1,0:T(8,128)(2,1)} %all-gather.4.cloned.1.call-done), kind=kLoop, calls=%fused_computation.51 | loop fusion | bytes 25165824 | tf_op jit(solution)/shard_map/split | solution.py:41
  112.0 18.8 %reshape.88 = bf16[16,768,4,64]{3,2,1,0:T(4,128)(2,1)} reshape(bf16[12288,256]{1,0:T(8,128)(2,1)} %get-tuple-element.249) | data formatting | bytes 12582912 | tf_op jit(solution)/shard_map/reshape | solution.py:90
  130.8 18.1 %copy.20 = bf16[16,768,4,64]{1,3,2,0:T(8,128)(2,1)} copy(bf16[16,768,4,64]{3,2,1,0:T(4,128)(2,1)} %reshape.88) | data formatting | bytes 12582912
  148.9 18.8 %reshape.89 = bf16[16,768,4,64]{3,2,1,0:T(4,128)(2,1)} reshape(bf16[12288,256]{1,0:T(8,128)(2,1)} %get-tuple-element.248) | data formatting | bytes 12582912 | tf_op jit(solution)/shard_map/reshape | solution.py:91
  167.7 18.1 %copy.21 = bf16[16,768,4,64]{1,3,2,0:T(8,128)(2,1)} copy(bf16[16,768,4,64]{3,2,1,0:T(4,128)(2,1)} %reshape.89) | data formatting | bytes 12582912
  185.8 33.7 %while.15 = (s32[]{:T(128)}, f32[4,768]{1,0:T(4,128)S(1)}, f32[4,768]{1,0:T(4,128)S(1)}, f32[768,4,64]{0,2,1:T(8,128)S(1)}, s32[16]{0:T(128)S(1)}, /*index=5*/s3...) while((s32[]{:T(128)}, f32[4,768]{1,0:T(4,128)S(1)}, ...), condition=%wide.region_5.6_spmd.clone, body=%wide.region_0.5_spmd.clone.sunk | while | flops 649800192 | bytes 33738040 | solution.py:127
  187.1 13.1 %conditional.3 = ((f32[4,768]{1,0:T(4,128)S(1)}, f32[4,768]{1,0:T(4,128)S(1)}, f32[768,4,64]{0,2,1:T(8,128)S(1)})) conditional(s32[]{:T(128)} %convert_element_type.100, (f32[4,768]{1,0:T(4,128)S(1)}, f32[4,768]{1,0:T(4,128)S(1)}, f32[768,4,64]{0,2,1:T(8,128)S(1)}) %tuple.41, (s32[]{:T(128)}, s32[]{:T(128)}, bf16[16,768,4,64]{1,3,2,0:T(8,128)(2,1)}, ...), branch_computations={%region_1.1_spmd, %region_2.4_spmd} | conditional | flops 649800192 | bytes 33734700 | solution.py:125
  188.2 3.9 fusion.4
  192.1 4.6 fusion.11
  196.7 3.5 fusion.3
  219.6 2.7 convolution_convert_fusion.1
  222.3 4.6 all-to-all-start.1
  227.6 37.7 %all-to-all-done.1 = bf16[8,96,2048]{2,1,0:T(8,128)(2,1)} async-done(((bf16[8,96,2048]{2,1,0:T(8,128)(2,1)}), bf16[8,96,2048]{2,1,0:T(8,128)(2,1)}, u32[]{:S(2)}, u32[]{:S(2)}) %all-to-all-start.1) | async-done | bytes 3145760 | tf_op jit(solution)/shard_map/all_to_all | solution.py:51
  265.3 2.5 reduce_sum.59
  271.6 2.1 stack.2
  273.7 4.4 all-to-all-start.2
  278.2 38.3 %all-to-all-done.2 = bf16[8,96,2048]{2,1,0:T(8,128)(2,1)} async-done(((bf16[8,96,2048]{2,1,0:T(8,128)(2,1)}), bf16[8,96,2048]{2,1,0:T(8,128)(2,1)}, u32[]{:S(2)}, u32[]{:S(2)}) %all-to-all-start.2) | async-done | bytes 3145760 | tf_op jit(solution)/shard_map/all_to_all | solution.py:13
  316.6 6.6 %fusion.27 = f32[768,704]{0,1:T(8,128)} fusion(bf16[768,2048]{1,0:T(8,128)(2,1)} %bitcast.12, bf16[2048,1408]{0,1:T(8,128)(2,1)} %all-gather.6.cloned.1.call-done), kind=kOutput, calls=%fused_computation.31 | convolution fusion | flops 2214592512 | bytes 8192000 | tf_op jit(solution)/shard_map/dot_general | solution.py:165
  323.1 152.3 %all-gather.8.cloned.1.call-done = bf16[704,2048]{1,0:T(8,128)(2,1)} async-done(((bf16[704,128]{1,0:T(8,128)(2,1)}), bf16[704,2048]{1,0:T(8,128)(2,1)}) %all-gather.8.cloned.1.call-update) | async-done | bytes 2883600 | tf_op jit(solution)/shard_map/all_gather | solution.py:170
  475.4 12.4 %convolution_convert_fusion = bf16[768,2048]{1,0:T(8,128)(2,1)} fusion(bf16[704,2048]{1,0:T(8,128)(2,1)} %all-gather.8.cloned.1.call-done, f32[768,704]{0,1:T(8,128)} %fusion.27, bf16[768,2048]{1,0:T(8,128)(2,1)} %bitcast.12, bf16[2048,1408]{0,1:T(8,128)(2,1)} %all-gather.6.cloned.1.call-done), kind=kOutput, calls=%fused_computation.27 | convolution fusion | flops 4434001920 | bytes 14221312 | tf_op jit(solution)/shard_map/dot_general | solution.py:168
  487.9 76.4 %reduce-scatter.2.cloned.1.call-done = bf16[96,2048]{1,0:T(8,128)(2,1)} async-done(((bf16[768,2048]{1,0:T(8,128)(2,1)}), bf16[96,2048]{1,0:T(8,128)(2,1)}) %reduce-scatter.2.cloned.1.call-update) | async-done | bytes 393232 | tf_op jit(solution)/shard_map/reduce_scatter | solution.py:173
  (93 shorter events, 24.7 us)
Async XLA Ops:
  6.5 213.1 %copy-start = (bf16[256,2048]{1,0:T(8,128)(2,1)S(1)}, bf16[256,2048]{1,0:T(8,128)(2,1)}, u32[]{:S(2)}) copy-start(bf16[256,2048]{1,0:T(8,128)(2,1)} %param.22) | copy-start | bytes 3145732
  6.5 95.4 %all-gather.4.cloned.1.call-start = ((), (), s32[]{:S(2)}) async-start(), calls=%async_computation.4 | async-start | bytes 13369344 | tf_op jit(solution)/shard_map/all_gather | solution.py:41
  8.8 269.4 %all-gather.6.cloned.1.call-start = ((), (), s32[]{:S(2)}) async-start(), calls=%async_computation.5 | async-start | bytes 6127616 | tf_op jit(solution)/shard_map/all_gather | solution.py:41
  12.0 173.7 %all-to-all-start = ((f32[16,768,4]{1,2,0:T(4,128)}), f32[16,768,4]{1,2,0:T(4,128)S(1)}, u32[]{:S(2)}, u32[]{:S(2)}) async-start(f32[16,768,4]{1,2,0:T(4,128)} %broadcast_in_dim.56), calls=%async_computation | async-start | bytes 393216 | tf_op jit(solution)/shard_map/all_to_all | solution.py:28
  167.7 18.2 %copy-start.1 = (f32[768,4]{0,1:T(4,128)S(1)}, f32[768,4]{0,1:T(4,128)}, u32[]{:S(2)}) copy-start(f32[768,4]{0,1:T(4,128)} %param.20) | copy-start | bytes 36868
  222.3 48.0 %copy-start.2 = (f32[2048]{0:T(1024)S(1)}, f32[2048]{0:T(1024)}, u32[]{:S(2)}) copy-start(f32[2048]{0:T(1024)} %param.24) | copy-start | bytes 24580
  222.3 48.0 %copy-start.3 = (f32[2048]{0:T(1024)S(1)}, f32[2048]{0:T(1024)}, u32[]{:S(2)}) copy-start(f32[2048]{0:T(1024)} %param.23) | copy-start | bytes 24580
  222.3 43.0 %all-to-all-start.1 = ((bf16[8,96,2048]{2,1,0:T(8,128)(2,1)}), bf16[8,96,2048]{2,1,0:T(8,128)(2,1)}, u32[]{:S(2)}, u32[]{:S(2)}) async-start(bf16[8,96,2048]{2,1,0:T(8,128)(2,1)} %bitcast.46), calls=%async_computation.1 | async-start | bytes 6291456 | tf_op jit(solution)/shard_map/all_to_all | solution.py:51
  226.9 248.5 %all-gather.8.cloned.1.call-start = ((), (), s32[]{:S(2)}) async-start(), calls=%async_computation.6 | async-start | bytes 3063808 | tf_op jit(solution)/shard_map/all_gather | solution.py:170
  273.7 42.9 %all-to-all-start.2 = ((bf16[8,96,2048]{2,1,0:T(8,128)(2,1)}), bf16[8,96,2048]{2,1,0:T(8,128)(2,1)}, u32[]{:S(2)}, u32[]{:S(2)}) async-start(bf16[8,96,2048]{2,1,0:T(8,128)(2,1)} %stack.2), calls=%async_computation.2 | async-start | bytes 6291456 | tf_op jit(solution)/shard_map/all_to_all | solution.py:13
  278.1 286.1 %reduce-scatter.2.cloned.1.call-start = ((), (), s32[]{:S(2)}) async-start(), calls=%async_computation.7 | async-start | bytes 3538944 | tf_op jit(solution)/shard_map/reduce_scatter | solution.py:173
  323.1 243.7 %copy-start.4 = (f32[2048]{0:T(1024)S(1)}, f32[2048]{0:T(1024)}, u32[]{:S(2)}) copy-start(f32[2048]{0:T(1024)} %param.29) | copy-start | bytes 24580
  323.1 243.7 %copy-start.5 = (f32[2048]{0:T(1024)S(1)}, f32[2048]{0:T(1024)}, u32[]{:S(2)}) copy-start(f32[2048]{0:T(1024)} %param.28) | copy-start | bytes 24580
Sparse Core Ops, SparseCore 0:
  9.5 92.3 all-gather.3
  104.0 64.0 all-gather.5
  229.8 245.5 all-gather.7
  488.0 76.1 reduce-scatter.1
